TPU v7x, 32 devices: a whole 2x2x4 slice. The times are simulated.
32 devices in a mesh: sp: 8 (over z, x), tp: 4 (over y, core).
Axes of the slice: x: 2, y: 2, z: 4, core: 2. Of those that a mesh axis runs over, the one named last changes fastest.
Arguments:
- tokens: bfloat16 [5120, 2048], P(('sp', 'tp')), may hold values from -44 to 44
- in_gain: float32 [2048], replicated, may hold values from 0.1 to 1.9
- w_x: bfloat16 [2048, 2048], P('sp', 'tp'), may hold values from -0.125 to 0.125
- w_z: bfloat16 [2048, 2048], P('sp', 'tp'), may hold values from -0.125 to 0.125
- w_b: bfloat16 [2048, 1024], P('sp', 'tp'), may hold values from -0.125 to 0.125
- w_c: bfloat16 [2048, 1024], P('sp', 'tp'), may hold values from -0.125 to 0.125
- w_dt: bfloat16 [2048, 32], replicated, may hold values from -0.125 to 0.125
- conv_x: float32 [4, 2048], replicated, may hold values from -3 to 3
- conv_b: float32 [4, 1024], replicated, may hold values from -3 to 3
- conv_c: float32 [4, 1024], replicated, may hold values from -3 to 3
- dt_bias: float32 [32], replicated, may hold values from -15 to -3.5
- a_log: float32 [32], replicated, may hold values from -0.5 to 0.5
- out_gain: float32 [2048], replicated, may hold values from 0.1 to 1.9
- w_out: bfloat16 [2048, 2048], P('tp', 'sp'), may hold values from -0.125 to 0.125
Outputs:
- mixer_out: bfloat16 [5120, 2048], P(('sp', 'tp'))
All inputs are finite; a program needn't handle non-finite values.
Results may differ from a plain program's by a relative error of at most 0.015.
Values may be sent and summed in bfloat16 or wider, within the bound.
A program may use at most 128 MiB of HBM per device.

v0:
```python
import jax
import jax.numpy as jnp
from jax import lax
from jax.sharding import PartitionSpec as P

HEAD_DIM = 64
STATE = 128
CONV = 4
BLOCK = 128
EPS = 1e-06
HIGH = lax.Precision.HIGHEST


def carried_in(part, axis, combine, identity):
    place = lax.axis_index(axis)
    gathered = jax.tree.map(lambda a: lax.all_gather(a, axis), part)
    state = jax.tree.map(lambda a, e: jnp.zeros_like(a) + jnp.asarray(e, a.dtype), part, identity)

    def one(lap, state):
        return combine(
            state, jax.tree.map(lambda a: lax.dynamic_index_in_dim(a, lap, 0, False), gathered)
        )

    return lax.fori_loop(0, place, one, state)


def from_behind(value, axis, steps):
    count = lax.axis_size(axis)
    first, last = (max(0, -steps), min(count, count - steps))
    return lax.ppermute(value, axis, [(source, source + steps) for source in range(first, last)])


def inverse_rms(values):
    return lax.rsqrt(jnp.mean(values * values, axis=-1, keepdims=True) + EPS)


def causal_conv(prev_rows, new_rows, kernel):
    joined = jnp.concatenate([prev_rows, new_rows], axis=0).astype(jnp.float32)
    row_count = new_rows.shape[0]
    summed = jnp.zeros(new_rows.shape, jnp.float32)
    for offset in range(kernel.shape[0]):
        summed = summed + kernel[offset] * joined[offset : offset + row_count]
    return jax.nn.silu(summed)


def fold_single(gathered):

    def fold_step(total_part, rows_part, first_row):
        return jnp.dot(gathered, rows_part, preferred_element_type=jnp.float32)

    return fold_step


def fold_products(gathered, totals, weight_rows, first_row):
    single = fold_single(gathered)
    return tuple(
        (
            single(total_part, rows_part, first_row)
            for total_part, rows_part in zip(totals, weight_rows)
        )
    )


def inner_part(cum_decay, b_rows, c_rows, scaled_x, causal):
    scores = jnp.einsum("blgn,bsgn->bgls", c_rows, b_rows, precision=HIGH)
    decay_gap = cum_decay[:, :, None] - cum_decay[:, None, :]
    causal_mask = causal[None, :, :, None, None]
    within = jnp.where(causal_mask, jnp.exp(jnp.where(causal_mask, decay_gap, 0.0)), 0.0)
    return jnp.einsum("bgls,blsgh,bsghp->blghp", scores, within, scaled_x, precision=HIGH)


def carried_part(c_rows, states, cum_decay):
    return jnp.einsum("blgn,bghpn,blgh->blghp", c_rows, states, jnp.exp(cum_decay), precision=HIGH)


def run_blocks(block_states, block_decay, start_state):

    def advance(run_state, inputs):
        fresh_state, factor = inputs
        return (run_state * factor[:, :, None, None] + fresh_state, run_state)

    final_state, entering = lax.scan(advance, start_state, (block_states, block_decay))
    return (entering, final_state)


def chain(earlier, later):
    return (earlier[0] * later[0], earlier[1] * later[0][:, :, None, None] + later[1])


def carry_in(total_decay, final_state):
    identity = (jnp.ones_like(total_decay), jnp.zeros_like(final_state))
    before = carried_in((total_decay, final_state), "sp", chain, identity)
    return before[1]


def body(
    tokens,
    in_gain,
    w_x,
    w_z,
    w_b,
    w_c,
    w_dt,
    conv_x,
    conv_b,
    conv_c,
    dt_bias,
    a_log,
    out_gain,
    w_out,
):
    share_index = lax.axis_index("tp")
    width_x = w_x.shape[1]
    width_b = w_b.shape[1]
    heads_here = width_x // HEAD_DIM
    groups_here = width_b // STATE
    group_heads = heads_here // groups_here
    kernel_x = lax.dynamic_slice_in_dim(conv_x, share_index * width_x, width_x, 1)
    kernel_b = lax.dynamic_slice_in_dim(conv_b, share_index * width_b, width_b, 1)
    kernel_c = lax.dynamic_slice_in_dim(conv_c, share_index * width_b, width_b, 1)
    bias_here = lax.dynamic_slice_in_dim(dt_bias, share_index * heads_here, heads_here, 0)
    rate_here = jnp.exp(lax.dynamic_slice_in_dim(a_log, share_index * heads_here, heads_here, 0))
    gain_here = lax.dynamic_slice_in_dim(out_gain, share_index * width_x, width_x, 0)
    dt_weight = lax.dynamic_slice_in_dim(w_dt, share_index * heads_here, heads_here, 1)
    values = tokens.astype(jnp.float32)
    normed = (values * inverse_rms(values) * in_gain).astype(jnp.bfloat16)
    gathered = lax.all_gather(normed, "tp", axis=0, tiled=True)
    seg_rows = gathered.shape[0]
    blocks = seg_rows // BLOCK
    empty_x = jnp.zeros((seg_rows, width_x), jnp.float32)
    empty_b = jnp.zeros((seg_rows, width_b), jnp.float32)
    projected = fold_products(
        gathered,
        (empty_x, empty_x, empty_b, empty_b),
        (
            lax.all_gather(w_x, "sp", axis=0, tiled=True),
            lax.all_gather(w_z, "sp", axis=0, tiled=True),
            lax.all_gather(w_b, "sp", axis=0, tiled=True),
            lax.all_gather(w_c, "sp", axis=0, tiled=True),
        ),
        jnp.int32(0),
    )
    proj_x, gate_rows, proj_b, proj_c = [
        summed_part.astype(jnp.bfloat16) for summed_part in projected
    ]
    dt_raw = jnp.dot(gathered, dt_weight, preferred_element_type=jnp.float32)
    conv_keep = CONV - 1
    tail_start = seg_rows - conv_keep
    prev_x, prev_b, prev_c = from_behind(
        (proj_x[tail_start:], proj_b[tail_start:], proj_c[tail_start:]), "sp", 1
    )
    conv_xs = causal_conv(prev_x, proj_x, kernel_x)
    conv_bs = causal_conv(prev_b, proj_b, kernel_b)
    conv_cs = causal_conv(prev_c, proj_c, kernel_c)
    step_size = jax.nn.softplus(dt_raw + bias_here)
    log_decay = (-step_size * rate_here).reshape(blocks, BLOCK, groups_here, group_heads)
    causal = lax.broadcasted_iota(jnp.int32, (BLOCK, BLOCK), 0) >= lax.broadcasted_iota(
        jnp.int32, (BLOCK, BLOCK), 1
    )
    cum_decay = jnp.einsum("ls,bsgh->blgh", causal.astype(jnp.float32), log_decay, precision=HIGH)
    scaled_x = (conv_xs.reshape(seg_rows, heads_here, HEAD_DIM) * step_size[:, :, None]).reshape(
        blocks, BLOCK, groups_here, group_heads, HEAD_DIM
    )
    b_rows = conv_bs.reshape(blocks, BLOCK, groups_here, STATE)
    c_rows = conv_cs.reshape(blocks, BLOCK, groups_here, STATE)
    block_total = cum_decay[:, BLOCK - 1]
    tail_weight = jnp.exp(block_total[:, None] - cum_decay)
    block_states = jnp.einsum(
        "blgn,blgh,blghp->bghpn", b_rows, tail_weight, scaled_x, precision=HIGH
    )
    block_decay = jnp.exp(block_total)
    total_decay = jnp.exp(jnp.sum(block_total, axis=0))
    start_state = jnp.zeros(block_states.shape[1:], jnp.float32)
    entering, final_state = run_blocks(block_states, block_decay, start_state)
    incoming = carry_in(total_decay, final_state)

    def per_block(run_state, inputs):
        cum_here, b_here, c_here, x_here, fresh_state, factor = inputs
        output = inner_part(cum_here[None], b_here[None], c_here[None], x_here[None], causal)[0]
        output = output + carried_part(c_here[None], run_state[None], cum_here[None])[0]
        return (run_state * factor[:, :, None, None] + fresh_state, output)

    unused, heads_out = lax.scan(
        per_block, incoming, (cum_decay, b_rows, c_rows, scaled_x, block_states, block_decay)
    )
    gated_out = heads_out.reshape(seg_rows, width_x) * jax.nn.silu(gate_rows.astype(jnp.float32))
    grouped = gated_out.reshape(seg_rows, groups_here, width_x // groups_here)
    mixed_rows = ((grouped * inverse_rms(grouped)).reshape(seg_rows, width_x) * gain_here).astype(
        jnp.bfloat16
    )
    partial_sum = jnp.dot(
        mixed_rows,
        lax.all_gather(w_out, "sp", axis=1, tiled=True),
        preferred_element_type=jnp.float32,
    )
    return lax.psum_scatter(partial_sum.astype(jnp.bfloat16), "tp", scatter_dimension=0, tiled=True)


def solution(mesh):
    in_specs = (
        P(("sp", "tp"), None),
        P(),
        P("sp", "tp"),
        P("sp", "tp"),
        P("sp", "tp"),
        P("sp", "tp"),
        P(),
        P(),
        P(),
        P(),
        P(),
        P(),
        P(),
        P("tp", "sp"),
    )
    out_specs = P(("sp", "tp"), None)
    return jax.shard_map(body, mesh=mesh, in_specs=in_specs, out_specs=out_specs, check_vma=False)
```

profile of v0, /device:TPU:0, one launch (start us, length us, event | category | flops | bytes accessed | tf_op | source)
XLA Modules:
  0.0 366.6 jit_solution(4335275581894576468)
XLA Ops:
  7.9 2.1 fusion.24
  14.8 23.7 %all-gather.11.cloned.1.call-done = bf16[640,2048]{1,0:T(8,128)(2,1)} async-done(((bf16[160,2048]{1,0:T(8,128)(2,1)}), bf16[640,2048]{1,0:T(8,128)(2,1)}) %all-gather.11.cloned.1.call-update) | async-done | bytes 2621456 | tf_op jit(solution)/shard_map/all_gather | solution.py:127
  38.5 2.7 negate_multiply_fusion
  42.1 38.8 %all-gather.15.cloned.1.call-done = bf16[2048,256]{1,0:T(8,128)(2,1)} async-done(((bf16[256,256]{1,0:T(8,128)(2,1)}), bf16[2048,256]{1,0:T(8,128)(2,1)}) %all-gather.15.cloned.1.call-update) | async-done | bytes 1048592 | tf_op jit(solution)/shard_map/all_gather | solution.py:138
  80.9 2.1 convolution_convert_fusion.4
  83.0 2.5 collective-permute-start.1
  85.5 45.4 %all-gather.13.cloned.1.call-done = bf16[2048,512]{1,0:T(8,128)(2,1)} async-done(((bf16[256,512]{1,0:T(8,128)(2,1)}), bf16[2048,512]{1,0:T(8,128)(2,1)}) %all-gather.13.cloned.1.call-update) | async-done | bytes 2097168 | tf_op jit(solution)/shard_map/all_gather | solution.py:136
  130.9 3.1 convolution_convert_fusion.2
  134.8 2.5 collective-permute-start
  151.1 20.7 %all-gather.17.cloned.1.call-done = bf16[2048,256]{1,0:T(8,128)(2,1)} async-done(((bf16[256,256]{1,0:T(8,128)(2,1)}), bf16[2048,256]{1,0:T(8,128)(2,1)}) %all-gather.17.cloned.1.call-update) | async-done | bytes 1048592 | tf_op jit(solution)/shard_map/all_gather | solution.py:139
  171.7 2.9 convolution_convert_fusion.3
  174.6 2.5 collective-permute-start.2
  177.1 17.5 %all-gather.2 = f32[8,2,4]{2,1,0:T(2,128)S(1)} all-gather(f32[1,2,4]{2,1,0:T(2,128)S(1)} %exponential_bitcast_fusion.1), channel_id=2, replica_groups=mesh['sp'=8,'tp'=4] {'sp'}, dimensions={0}, use_global_device_ids=true | all-gather | bytes 288 | tf_op jit(solution)/shard_map/all_gather | solution.py:16
  197.4 24.2 %all-gather.23.cloned.1.call-done = f32[16,4,64,128]{3,2,1,0:T(8,128)} async-done(((f32[2,4,64,128]{3,2,1,0:T(8,128)}), f32[16,4,64,128]{3,2,1,0:T(8,128)}) %all-gather.23.cloned.1.call-update) | async-done | bytes 2097168 | tf_op jit(solution)/shard_map/all_gather | solution.py:16
  221.8 24.1 %while.38 = (s32[]{:T(128)}, f32[2,4,64,128]{3,2,1,0:T(8,128)S(1)}, f32[5,128,2,4,64]{1,4,3,2,0:T(8,128)}, f32[5,2,4]{2,1,0:T(2,128)S(1)}, f32[5,2,4,64,128]{4,3...) while((s32[]{:T(128)}, f32[2,4,64,128]{3,2,1,0:T(8,128)S(1)}, ...), condition=%wide.region_7.8_spmd.clone.clone, body=%wide.region_6.7_spmd.clone.clone.sunk | while | flops 252461056 | bytes 3863257 | solution.py:183
  229.4 1.9 fusion.77
  243.8 1.9 fusion.77
  245.9 3.0 copy.89
  248.9 2.8 reshape.123
  251.7 19.6 %all-gather.19.cloned.1.call-done = bf16[2048,512]{1,0:T(8,128)(2,1)} async-done(((bf16[256,512]{1,0:T(8,128)(2,1)}), bf16[2048,512]{1,0:T(8,128)(2,1)}) %all-gather.19.cloned.1.call-update) | async-done | bytes 2097168 | tf_op jit(solution)/shard_map/all_gather | solution.py:137
  271.3 5.5 %fusion.49 = (f32[640,512]{1,0:T(8,128)S(1)}, f32[640,512]{1,0:T(8,128)}) fusion(f32[640,512]{1,0:T(8,128)} %reshape.123, bf16[640,2048]{1,0:T(8,128)(2,1)} %all-gather.11.cloned.1.call-done, bf16[2048,512]{1,0:T(8,128)(2,1)} %all-gather.19.cloned.1.call-done), kind=kOutput, calls=%fused_computation.107 | convolution fusion | flops 1344798720 | bytes 8650752 | tf_op jit(solution)/shard_map/dot_general | solution.py:49
  279.5 42.8 %all-gather.21.cloned.1.call-done = bf16[512,2048]{1,0:T(8,128)(2,1)} async-done(((bf16[512,256]{1,0:T(8,128)(2,1)}), bf16[512,2048]{1,0:T(8,128)(2,1)}) %all-gather.21.cloned.1.call-update) | async-done | bytes 2097168 | tf_op jit(solution)/shard_map/all_gather | solution.py:193
  322.3 4.6 %convolution_convert_fusion = bf16[640,2048]{1,0:T(8,128)(2,1)} fusion(bf16[512,2048]{1,0:T(8,128)(2,1)} %all-gather.21.cloned.1.call-done, f32[640,512]{1,0:T(8,128)S(1)} %copy-done.11, f32[640,512]{1,0:T(8,128)S(1)} %bitcast.131, f32[512]{0:T(512)S(1)} %dynamic_slice.66), kind=kOutput, calls=%fused_computation.38 | convolution fusion | flops 1344471040 | bytes 7342080 | tf_op jit(solution)/shard_map/dot_general | solution.py:191
  326.9 32.8 %reduce-scatter.2.cloned.1.call-done = bf16[160,2048]{1,0:T(8,128)(2,1)} async-done(((bf16[640,2048]{1,0:T(8,128)(2,1)}), bf16[160,2048]{1,0:T(8,128)(2,1)}) %reduce-scatter.2.cloned.1.call-update) | async-done | bytes 655376 | tf_op jit(solution)/shard_map/reduce_scatter | solution.py:196
  (141 shorter events, 47.3 us)
Async XLA Ops:
  6.5 32.0 %copy-start = (bf16[2048,32]{0,1:T(8,128)(2,1)S(1)}, bf16[2048,32]{0,1:T(8,128)(2,1)}, u32[]{:S(2)}) copy-start(bf16[2048,32]{0,1:T(8,128)(2,1)} %param.26) | copy-start | bytes 393220
  6.5 32.0 %all-gather.11.cloned.1.call-start = ((), (), s32[]{:S(2)}) async-start(), calls=%async_computation.1 | async-start | bytes 3276800 | tf_op jit(solution)/shard_map/all_gather | solution.py:127
  7.9 4.3 %copy-start.9 = (f32[32]{0:T(128)S(1)}, f32[32]{0:T(128)}, u32[]{:S(2)}) copy-start(f32[32]{0:T(128)} %param.31) | copy-start | bytes 388
  7.9 4.4 %copy-start.10 = (f32[32]{0:T(128)S(1)}, f32[32]{0:T(128)}, u32[]{:S(2)}) copy-start(f32[32]{0:T(128)} %param.30) | copy-start | bytes 388
  10.1 70.8 %all-gather.15.cloned.1.call-start = ((), (), s32[]{:S(2)}) async-start(), calls=%async_computation.3 | async-start | bytes 1179648 | tf_op jit(solution)/shard_map/all_gather | solution.py:138
  10.8 120.1 %all-gather.13.cloned.1.call-start = ((), (), s32[]{:S(2)}) async-start(), calls=%async_computation.2 | async-start | bytes 2359296 | tf_op jit(solution)/shard_map/all_gather | solution.py:136
  11.6 160.2 %all-gather.17.cloned.1.call-start = ((), (), s32[]{:S(2)}) async-start(), calls=%async_computation.4 | async-start | bytes 1179648 | tf_op jit(solution)/shard_map/all_gather | solution.py:139
  12.1 209.4 %all-gather.23.cloned.1.call-start = ((), (), s32[]{:S(2)}) async-start(), calls=%async_computation.8 | async-start | bytes 2359296 | tf_op jit(solution)/shard_map/all_gather | solution.py:16
  38.5 42.4 %copy-start.2 = (bf16[640,2048]{1,0:T(8,128)(2,1)S(1)}, bf16[640,2048]{1,0:T(8,128)(2,1)}, u32[]{:S(2)}) copy-start(bf16[640,2048]{1,0:T(8,128)(2,1)} %all-gather.11.cloned.1.call-done) | copy-start | bytes 7864324
  83.0 55.0 %collective-permute-start.1 = (bf16[3,256]{1,0:T(4,128)(2,1)S(1)}, bf16[3,256]{1,0:T(4,128)(2,1)S(1)}, u32[]{:S(2)}, u32[]{:S(2)}) collective-permute-start(bf16[3,256]{1,0:T(4,128)(2,1)S(1)} %slice.118), channel_id=1, source_target_pairs={{0,4},{4,8},{8,12},{12,16},{16,20},{20,24},{24,28},{1,5},{5,9},{9,... | collective-permute-start | bytes 4616 | tf_op jit(solution)/shard_map/ppermute | solution.py:30
  134.0 0.8 copy-start.3
  134.8 4.0 %collective-permute-start = (bf16[3,512]{1,0:T(4,128)(2,1)S(1)}, bf16[3,512]{1,0:T(4,128)(2,1)S(1)}, u32[]{:S(2)}, u32[]{:S(2)}) collective-permute-start(bf16[3,512]{1,0:T(4,128)(2,1)S(1)} %slice.113), channel_id=1, source_target_pairs={{0,4},{4,8},{8,12},{12,16},{16,20},{20,24},{24,28},{1,5},{5,9},{9,... | collective-permute-start | bytes 9224 | tf_op jit(solution)/shard_map/ppermute | solution.py:30
  138.5 1.1 copy-start.4
  138.8 0.9 copy-start.6
  138.9 0.9 copy-start.7
  142.1 1.4 copy-start.5
  147.3 0.7 copy-start.1
  148.0 123.3 %all-gather.19.cloned.1.call-start = ((), (), s32[]{:S(2)}) async-start(), calls=%async_computation.5 | async-start | bytes 2359296 | tf_op jit(solution)/shard_map/all_gather | solution.py:137
  148.6 173.7 %all-gather.21.cloned.1.call-start = ((), (), s32[]{:S(2)}) async-start(), calls=%async_computation.6 | async-start | bytes 2359296 | tf_op jit(solution)/shard_map/all_gather | solution.py:193
  149.3 210.4 %reduce-scatter.2.cloned.1.call-start = ((), (), s32[]{:S(2)}) async-start(), calls=%async_computation.7 | async-start | bytes 3276800 | tf_op jit(solution)/shard_map/reduce_scatter | solution.py:196
  151.1 26.0 %copy-start.8 = (f32[2,4]{1,0:T(2,128)S(1)}, f32[2,4]{1,0:T(2,128)}, u32[]{:S(2)}) copy-start(f32[2,4]{1,0:T(2,128)} %get-tuple-element.254) | copy-start | bytes 100
  174.6 20.1 %collective-permute-start.2 = (bf16[3,256]{1,0:T(4,128)(2,1)S(1)}, bf16[3,256]{1,0:T(4,128)(2,1)S(1)}, u32[]{:S(2)}, u32[]{:S(2)}) collective-permute-start(bf16[3,256]{1,0:T(4,128)(2,1)S(1)} %slice.123), channel_id=1, source_target_pairs={{0,4},{4,8},{8,12},{12,16},{16,20},{20,24},{24,28},{1,5},{5,9},{9,... | collective-permute-start | bytes 4616 | tf_op jit(solution)/shard_map/ppermute | solution.py:30
  279.4 42.9 %copy-start.11 = (f32[640,512]{1,0:T(8,128)S(1)}, f32[640,512]{1,0:T(8,128)}, u32[]{:S(2)}) copy-start(f32[640,512]{1,0:T(8,128)} %get-tuple-element.310) | copy-start | bytes 3932164
Sparse Core Ops, SparseCore 0:
  10.2 28.2 all-gather.10
  40.6 40.2 all-gather.14
  83.0 47.7 all-gather.12
  132.9 38.8 all-gather.16
  173.7 47.8 all-gather.22
  223.5 47.7 all-gather.18
  273.3 48.8 all-gather.20
  327.0 32.6 reduce-scatter.1
where the time goes:
time: 368 us; the launch traced here: 367 us
  waiting for transfers between devices  251 us (68%)
  matrix products  36 us (10%)
  local copies, waits for them, and re-layouts  29 us (8%)
  blocking collectives  17.5 us (5%)
  between operations  13.9 us (4%)
  other arithmetic  10.7 us (3%)
  starting transfers between devices  7.7 us (2%)
    all_gather x1, waiting for transfers between devices, body(): lax.all_gather(w_x, 'sp', axis=0, tiled=True)  45.4 us
    all_gather x1, waiting for transfers between devices, body(): lax.all_gather(w_out, 'sp', axis=1, tiled=True)  42.8 us
    all_gather x1, waiting for transfers between devices, body(): lax.all_gather(w_b, 'sp', axis=0, tiled=True)  38.8 us
    reduce_scatter x1, waiting for transfers between devices, body(): lax.psum_scatter(partial_sum.astype(jnp.bfloat16), 'tp', scatter_dimensio...  32.8 us
    all_gather x1, waiting for transfers between devices, carried_in(): gathered = jax.tree.map(lambda a: lax.all_gather(a, axis), part)  24.2 us
    all_gather x1, waiting for transfers between devices, body(): gathered = lax.all_gather(normed, 'tp', axis=0, tiled=True)  23.7 us
    all_gather x1, waiting for transfers between devices, body(): lax.all_gather(w_c, 'sp', axis=0, tiled=True)  20.7 us
    all_gather x1, waiting for transfers between devices, body(): lax.all_gather(w_z, 'sp', axis=0, tiled=True)  19.6 us
  transfers between devices with their start and end apart: 11, of which 8 were waited for; matrix products, arithmetic and copies ran while one was open for 18% of the time, Pallas kernels for 0%

commit v1 on v0

--- a/solution.py
+++ b/solution.py
@@ -124,7 +124,19 @@
     dt_weight = lax.dynamic_slice_in_dim(w_dt, share_index * heads_here, heads_here, 1)
     values = tokens.astype(jnp.float32)
     normed = (values * inverse_rms(values) * in_gain).astype(jnp.bfloat16)
-    gathered = lax.all_gather(normed, "tp", axis=0, tiled=True)
+    table = []
+    ix = 0
+    axis_len = lax.axis_size("tp")
+    while ix < axis_len:
+        table.append((ix, (ix + 1) % axis_len))
+        ix = ix + 1
+    next_value = [None] * axis_len
+    next_value[axis_len - 1] = normed
+    for j in range(axis_len - 2, -1, -1):
+        next_value[j] = lax.ppermute(next_value[j + 1], "tp", table)
+    gathered = jnp.roll(
+        jnp.concatenate(next_value, 0), (lax.axis_index("tp") + 1) * normed.shape[0], 0
+    )
     seg_rows = gathered.shape[0]
     blocks = seg_rows // BLOCK
     empty_x = jnp.zeros((seg_rows, width_x), jnp.float32)

time: 368 us -> 339 us (0.921)
  waiting for transfers between devices: 251 us -> 216 us
    all_gather x1, waiting for transfers between devices: 38.8 us -> 3.88 us  [body(): lax.all_gather(w_b, 'sp', axis=0, tiled=True)]
    ppermute x0 -> x3, waiting for transfers between devices: none -> 28.1 us  [body(): next_value[j] = lax.ppermute(next_value[j + 1], 'tp', table)]
    all_gather x1 -> x0, waiting for transfers between devices: 23.7 us -> none  [body(): gathered = lax.all_gather(normed, 'tp', axis=0, tiled=True)]
    all_gather x1, waiting for transfers between devices: 45.4 us -> 41.3 us  [body(): lax.all_gather(w_x, 'sp', axis=0, tiled=True)]
    unnamed x27 -> x23, local copies, waits for them, and re-layouts: 2.37 us -> 6.3 us
  transfers between devices with their start and end apart: 11 -> 13, of which waited for: 8 -> 11; matrix products, arithmetic and copies ran while one was open for 18% -> 23% of each run, Pallas kernels for 0% -> 0%
where the time goes in v1:
time: 339 us; the launch traced here: 338 us
  waiting for transfers between devices  216 us (64%)
  matrix products  37.6 us (11%)
  local copies, waits for them, and re-layouts  31.1 us (9%)
  blocking collectives  17.5 us (5%)
  between operations  13.8 us (4%)
  other arithmetic  13 us (4%)
  starting transfers between devices  8.23 us (2%)
    all_gather x1, waiting for transfers between devices, body(): lax.all_gather(w_out, 'sp', axis=1, tiled=True)  42.6 us
    all_gather x1, waiting for transfers between devices, body(): lax.all_gather(w_x, 'sp', axis=0, tiled=True)  41.3 us
    reduce_scatter x1, waiting for transfers between devices, body(): lax.psum_scatter(partial_sum.astype(jnp.bfloat16), 'tp', scatter_dimensio...  32.8 us
    ppermute x3, waiting for transfers between devices, body(): next_value[j] = lax.ppermute(next_value[j + 1], 'tp', table)  28.1 us
    all_gather x1, waiting for transfers between devices, carried_in(): gathered = jax.tree.map(lambda a: lax.all_gather(a, axis), part)  26.1 us
    all_gather x1, waiting for transfers between devices, body(): lax.all_gather(w_z, 'sp', axis=0, tiled=True)  19.6 us
    all_gather x1, waiting for transfers between devices, body(): lax.all_gather(w_c, 'sp', axis=0, tiled=True)  18.7 us
    all_gather x1, blocking collectives, carried_in(): gathered = jax.tree.map(lambda a: lax.all_gather(a, axis), part)  17.5 us
  transfers between devices with their start and end apart: 13, of which 11 were waited for; matrix products, arithmetic and copies ran while one was open for 23% of the time, Pallas kernels for 0%

profile of v1, /device:TPU:0, one launch (start us, length us, event | category | flops | bytes accessed | tf_op | source)
XLA Modules:
  0.0 338.2 jit_solution(3468025172702865657)
XLA Ops:
  10.8 10.2 %collective-permute-done = bf16[160,2048]{1,0:T(8,128)(2,1)S(1)} collective-permute-done((bf16[160,2048]{1,0:T(8,128)(2,1)S(1)}, bf16[160,2048]{1,0:T(8,128)(2,1)S(1)}, u32[]{:S(2)}, u32[]{:S(2)}) %collective-permute-start) | collective-permute-done | bytes 655392 | tf_op jit(solution)/shard_map/ppermute | solution.py:136
  21.1 10.0 %collective-permute-done.1 = bf16[160,2048]{1,0:T(8,128)(2,1)S(1)} collective-permute-done((bf16[160,2048]{1,0:T(8,128)(2,1)S(1)}, bf16[160,2048]{1,0:T(8,128)(2,1)S(1)}, u32[]{:S(2)}, u32[]{:S(2)}) %collective-permute-start.1) | collective-permute-done | bytes 655392 | tf_op jit(solution)/shard_map/ppermute | solution.py:136
  33.2 7.9 %collective-permute-done.2 = bf16[160,2048]{1,0:T(8,128)(2,1)S(1)} collective-permute-done((bf16[160,2048]{1,0:T(8,128)(2,1)S(1)}, bf16[160,2048]{1,0:T(8,128)(2,1)S(1)}, u32[]{:S(2)}, u32[]{:S(2)}) %collective-permute-start.2) | collective-permute-done | bytes 655392 | tf_op jit(solution)/shard_map/ppermute | solution.py:136
  48.6 3.9 %all-gather.12.cloned.1.call-done = bf16[2048,256]{1,0:T(8,128)(2,1)} async-done(((bf16[256,256]{1,0:T(8,128)(2,1)}), bf16[2048,256]{1,0:T(8,128)(2,1)}) %all-gather.12.cloned.1.call-update) | async-done | bytes 1048592 | tf_op jit(solution)/shard_map/all_gather | solution.py:150
  52.5 2.9 fusion.50
  55.4 2.5 collective-permute-start.4
  57.9 2.6 negate_multiply_fusion
  61.2 41.3 %all-gather.10.cloned.1.call-done = bf16[2048,512]{1,0:T(8,128)(2,1)} async-done(((bf16[256,512]{1,0:T(8,128)(2,1)}), bf16[2048,512]{1,0:T(8,128)(2,1)}) %all-gather.10.cloned.1.call-update) | async-done | bytes 2097168 | tf_op jit(solution)/shard_map/all_gather | solution.py:148
  102.5 3.9 %fusion.32 = bf16[640,512]{1,0:T(8,128)(2,1)S(1)} fusion(bf16[2048,512]{1,0:T(8,128)(2,1)} %all-gather.10.cloned.1.call-done, bf16[1280,2048]{1,0:T(8,128)(2,1)} %constant_dynamic-update-slice_fusion, s32[]{:T(128)S(6)} %select_n.51), kind=kOutput, calls=%fused_computation.53 | convolution fusion | flops 1342504960 | bytes 5373956 | tf_op jit(solution)/shard_map/dot_general | solution.py:49
  106.4 2.4 collective-permute-start.3
  115.5 3.5 %broadcast_multiply_fusion.1 = (f32[5,128,2,4,64]{1,0,4,3,2:T(8,128)S(1)}, f32[5,128,2,4,64]{1,0,4,3,2:T(8,128)}) fusion(f32[5,128,2,4]{1,0,3,2:T(8,128)S(1)} %subtract_exponential_fusion, f32[5,128,2,4,64]{1,0,4,3,2:T(8,128)} %reshape.103, f32[5,128,2,4]{1,0,3,2:T(8,128)S(1)} %copy.69), kind=kLoop, calls=%fused_computation.78 | loop fusion | flops 655360 | bytes 3973120 | tf_op jit(solution)/shard_map/blgn,blgh,blghp->bghpn/dot_general | solution.py:180
  124.7 18.7 %all-gather.14.cloned.1.call-done = bf16[2048,256]{1,0:T(8,128)(2,1)} async-done(((bf16[256,256]{1,0:T(8,128)(2,1)}), bf16[2048,256]{1,0:T(8,128)(2,1)}) %all-gather.14.cloned.1.call-update) | async-done | bytes 1048592 | tf_op jit(solution)/shard_map/all_gather | solution.py:151
  143.4 2.9 fusion.53
  146.3 2.5 collective-permute-start.5
  148.8 17.5 %all-gather.2 = f32[8,2,4]{2,1,0:T(2,128)S(1)} all-gather(f32[1,2,4]{2,1,0:T(2,128)S(1)} %exponential_bitcast_fusion.1), channel_id=2, replica_groups=mesh['sp'=8,'tp'=4] {'sp'}, dimensions={0}, use_global_device_ids=true | all-gather | bytes 288 | tf_op jit(solution)/shard_map/all_gather | solution.py:16
  167.2 26.1 %all-gather.20.cloned.1.call-done = f32[16,4,64,128]{3,2,1,0:T(8,128)} async-done(((f32[2,4,64,128]{3,2,1,0:T(8,128)}), f32[16,4,64,128]{3,2,1,0:T(8,128)}) %all-gather.20.cloned.1.call-update) | async-done | bytes 2097168 | tf_op jit(solution)/shard_map/all_gather | solution.py:16
  193.5 24.1 %while.38 = (s32[]{:T(128)}, f32[2,4,64,128]{3,2,1,0:T(8,128)S(1)}, f32[5,128,2,4,64]{1,4,3,2,0:T(8,128)}, f32[5,2,4]{2,1,0:T(2,128)S(1)}, f32[5,2,4,64,128]{4,3...) while((s32[]{:T(128)}, f32[2,4,64,128]{3,2,1,0:T(8,128)S(1)}, ...), condition=%wide.region_7.8_spmd.clone.clone, body=%wide.region_6.7_spmd.clone.clone.sunk | while | flops 252461056 | bytes 3863257 | solution.py:195
  217.6 3.0 copy.89
  220.7 2.7 reshape.123
  223.4 19.6 %all-gather.16.cloned.1.call-done = bf16[2048,512]{1,0:T(8,128)(2,1)} async-done(((bf16[256,512]{1,0:T(8,128)(2,1)}), bf16[2048,512]{1,0:T(8,128)(2,1)}) %all-gather.16.cloned.1.call-update) | async-done | bytes 2097168 | tf_op jit(solution)/shard_map/all_gather | solution.py:149
  243.0 5.6 %fusion.82 = (f32[640,512]{1,0:T(8,128)S(1)}, f32[640,512]{1,0:T(8,128)}) fusion(f32[640,512]{1,0:T(8,128)} %reshape.123, bf16[2048,512]{1,0:T(8,128)(2,1)} %all-gather.16.cloned.1.call-done, bf16[1280,2048]{1,0:T(8,128)(2,1)} %constant_dynamic-update-slice_fusion, s32[]{:T(128)S(6)} %select_n.51), kind=kOutput, calls=%fused_computation.129 | convolution fusion | flops 1344798720 | bytes 8650756 | tf_op jit(solution)/shard_map/dot_general | solution.py:49
  251.2 42.6 %all-gather.18.cloned.1.call-done = bf16[512,2048]{1,0:T(8,128)(2,1)} async-done(((bf16[512,256]{1,0:T(8,128)(2,1)}), bf16[512,2048]{1,0:T(8,128)(2,1)}) %all-gather.18.cloned.1.call-update) | async-done | bytes 2097168 | tf_op jit(solution)/shard_map/all_gather | solution.py:205
  293.8 4.6 %convolution_convert_fusion = bf16[640,2048]{1,0:T(8,128)(2,1)} fusion(bf16[512,2048]{1,0:T(8,128)(2,1)} %all-gather.18.cloned.1.call-done, f32[640,512]{1,0:T(8,128)S(1)} %copy-done.6, f32[640,512]{1,0:T(8,128)S(1)} %bitcast.126, f32[512]{0:T(512)S(1)} %dynamic_slice.71), kind=kOutput, calls=%fused_computation.38 | convolution fusion | flops 1344471040 | bytes 7342080 | tf_op jit(solution)/shard_map/dot_general | solution.py:203
  298.5 32.8 %reduce-scatter.2.cloned.1.call-done = bf16[160,2048]{1,0:T(8,128)(2,1)} async-done(((bf16[640,2048]{1,0:T(8,128)(2,1)}), bf16[160,2048]{1,0:T(8,128)(2,1)}) %reduce-scatter.2.cloned.1.call-update) | async-done | bytes 655376 | tf_op jit(solution)/shard_map/reduce_scatter | solution.py:208
  (142 shorter events, 54.8 us)
Async XLA Ops:
  6.5 51.4 %copy-start = (bf16[2048,32]{0,1:T(8,128)(2,1)S(1)}, bf16[2048,32]{0,1:T(8,128)(2,1)}, u32[]{:S(2)}) copy-start(bf16[2048,32]{0,1:T(8,128)(2,1)} %param.26) | copy-start | bytes 393220
  6.5 2.8 copy-start.1
  6.5 24.7 %copy-start.4 = (f32[32]{0:T(128)S(1)}, f32[32]{0:T(128)}, u32[]{:S(2)}) copy-start(f32[32]{0:T(128)} %param.30) | copy-start | bytes 388
  6.5 24.7 %copy-start.5 = (f32[32]{0:T(128)S(1)}, f32[32]{0:T(128)}, u32[]{:S(2)}) copy-start(f32[32]{0:T(128)} %param.31) | copy-start | bytes 388
  6.5 46.0 %all-gather.12.cloned.1.call-start = ((), (), s32[]{:S(2)}) async-start(), calls=%async_computation.2 | async-start | bytes 1179648 | tf_op jit(solution)/shard_map/all_gather | solution.py:150
  7.3 95.2 %all-gather.10.cloned.1.call-start = ((), (), s32[]{:S(2)}) async-start(), calls=%async_computation.1 | async-start | bytes 2359296 | tf_op jit(solution)/shard_map/all_gather | solution.py:148
  8.0 135.4 %all-gather.14.cloned.1.call-start = ((), (), s32[]{:S(2)}) async-start(), calls=%async_computation.3 | async-start | bytes 1179648 | tf_op jit(solution)/shard_map/all_gather | solution.py:151
  10.3 10.8 %collective-permute-start = (bf16[160,2048]{1,0:T(8,128)(2,1)S(1)}, bf16[160,2048]{1,0:T(8,128)(2,1)S(1)}, u32[]{:S(2)}, u32[]{:S(2)}) collective-permute-start(bf16[160,2048]{1,0:T(8,128)(2,1)S(1)} %fusion.40), channel_id=1, source_target_pairs={{0,1},{1,2},{2,3},{3,0},{4,5},{5,6},{6,7},{7,4},{8,9},{9,10},{10,1... | collective-permute-start | bytes 1966088 | tf_op jit(solution)/shard_map/ppermute | solution.py:136
  21.1 10.0 %collective-permute-start.1 = (bf16[160,2048]{1,0:T(8,128)(2,1)S(1)}, bf16[160,2048]{1,0:T(8,128)(2,1)S(1)}, u32[]{:S(2)}, u32[]{:S(2)}) collective-permute-start(bf16[160,2048]{1,0:T(8,128)(2,1)S(1)} %collective-permute-done), channel_id=1, source_target_pairs={{0,1},{1,2},{2,3},{3,0},{4,5},{5,6},{6,7},{7,4},{8,9},{9,10},{10,1... | collective-permute-start | bytes 1966088 | tf_op jit(solution)/shard_map/ppermute | solution.py:136
  31.1 10.0 %collective-permute-start.2 = (bf16[160,2048]{1,0:T(8,128)(2,1)S(1)}, bf16[160,2048]{1,0:T(8,128)(2,1)S(1)}, u32[]{:S(2)}, u32[]{:S(2)}) collective-permute-start(bf16[160,2048]{1,0:T(8,128)(2,1)S(1)} %collective-permute-done.1), channel_id=1, source_target_pairs={{0,1},{1,2},{2,3},{3,0},{4,5},{5,6},{6,7},{7,4},{8,9},{9,10},{10,1... | collective-permute-start | bytes 1966088 | tf_op jit(solution)/shard_map/ppermute | solution.py:136
  31.1 162.2 %all-gather.20.cloned.1.call-start = ((), (), s32[]{:S(2)}) async-start(), calls=%async_computation.7 | async-start | bytes 2359296 | tf_op jit(solution)/shard_map/all_gather | solution.py:16
  42.0 1.8 copy-start.3
  55.4 5.7 %collective-permute-start.4 = (bf16[3,256]{1,0:T(4,128)(2,1)S(1)}, bf16[3,256]{1,0:T(4,128)(2,1)S(1)}, u32[]{:S(2)}, u32[]{:S(2)}) collective-permute-start(bf16[3,256]{1,0:T(4,128)(2,1)S(1)} %slice.118), channel_id=1, source_target_pairs={{0,4},{4,8},{8,12},{12,16},{16,20},{20,24},{24,28},{1,5},{5,9},{9,... | collective-permute-start | bytes 4616 | tf_op jit(solution)/shard_map/ppermute | solution.py:30
  106.4 3.8 %collective-permute-start.3 = (bf16[3,512]{1,0:T(4,128)(2,1)S(1)}, bf16[3,512]{1,0:T(4,128)(2,1)S(1)}, u32[]{:S(2)}, u32[]{:S(2)}) collective-permute-start(bf16[3,512]{1,0:T(4,128)(2,1)S(1)} %slice.113), channel_id=1, source_target_pairs={{0,4},{4,8},{8,12},{12,16},{16,20},{20,24},{24,28},{1,5},{5,9},{9,... | collective-permute-start | bytes 9224 | tf_op jit(solution)/shard_map/ppermute | solution.py:30
  121.1 0.7 copy-start.2
  121.8 121.2 %all-gather.16.cloned.1.call-start = ((), (), s32[]{:S(2)}) async-start(), calls=%async_computation.4 | async-start | bytes 2359296 | tf_op jit(solution)/shard_map/all_gather | solution.py:149
  122.4 171.4 %all-gather.18.cloned.1.call-start = ((), (), s32[]{:S(2)}) async-start(), calls=%async_computation.5 | async-start | bytes 2359296 | tf_op jit(solution)/shard_map/all_gather | solution.py:205
  123.0 208.3 %reduce-scatter.2.cloned.1.call-start = ((), (), s32[]{:S(2)}) async-start(), calls=%async_computation.6 | async-start | bytes 3276800 | tf_op jit(solution)/shard_map/reduce_scatter | solution.py:208
  146.3 20.0 %collective-permute-start.5 = (bf16[3,256]{1,0:T(4,128)(2,1)S(1)}, bf16[3,256]{1,0:T(4,128)(2,1)S(1)}, u32[]{:S(2)}, u32[]{:S(2)}) collective-permute-start(bf16[3,256]{1,0:T(4,128)(2,1)S(1)} %slice.123), channel_id=1, source_target_pairs={{0,4},{4,8},{8,12},{12,16},{16,20},{20,24},{24,28},{1,5},{5,9},{9,... | collective-permute-start | bytes 4616 | tf_op jit(solution)/shard_map/ppermute | solution.py:30
  251.1 42.8 %copy-start.6 = (f32[640,512]{1,0:T(8,128)S(1)}, f32[640,512]{1,0:T(8,128)}, u32[]{:S(2)}) copy-start(f32[640,512]{1,0:T(8,128)} %get-tuple-element.310) | copy-start | bytes 3932164
Sparse Core Ops, SparseCore 0:
  9.5 42.9 all-gather.11
  54.6 47.7 all-gather.9
  104.6 38.7 all-gather.13
  145.4 47.8 all-gather.19
  195.2 47.7 all-gather.15
  244.9 48.8 all-gather.17
  298.6 32.6 reduce-scatter.1
